TPU v7x, 32 devices: a whole 2x2x4 slice. The times are simulated.
32 devices in a mesh: sp: 8 (over z, x), tp: 4 (over y, core).
Axes of the slice: x: 2, y: 2, z: 4, core: 2. Of those that a mesh axis runs over, the one named last changes fastest.
Arguments:
- queries: bfloat16 [3072, 1024], P('sp', 'tp'), may hold values from -160 to 160
- key_vectors: bfloat16 [3072, 1024], P('sp', 'tp'), may hold values from -7 to 7
- values: bfloat16 [3072, 1024], P('sp', 'tp'), may hold values from -6 to 6
- head_lambda: float32 [8], P('tp'), may hold values from 0.3 to 0.8
- head_gain: float32 [128], replicated, may hold values from 0.1 to 1.9
- w_out: bfloat16 [1024, 2048], P('tp'), may hold values from -0.1875 to 0.1875
- residual: bfloat16 [3072, 2048], P(('sp', 'tp')), may hold values from -6 to 6
- ffn_gain: float32 [2048], replicated, may hold values from 0.1 to 1.9
- route_ids: int32 [3072, 2], P(('sp', 'tp')), may hold values from 0 to 7, all different within a row; in each aligned block of 96 rows (0 to 95, 96 to 191, ...) at most 30 rows name the same one
- route_logits: float32 [3072, 2], P(('sp', 'tp')), may hold values from -8 to 310
- w_gate: bfloat16 [8, 2048, 2048], P('sp', None, 'tp'), may hold values from -0.3125 to 0.3125
- w_up: bfloat16 [8, 2048, 2048], P('sp', None, 'tp'), may hold values from -0.3125 to 0.3125
- w_down: bfloat16 [8, 2048, 2048], P('sp', 'tp'), may hold values from -0.125 to 0.125
Outputs:
- layer_out: bfloat16 [3072, 2048], P(('sp', 'tp'))
Inputs may be any that keep to these rules, and one draw needn't show every extreme that they name: `route_ids`: in the rows of one device after the attention (aligned blocks of 96 rows) no expert is named by more than 30 rows, a bound that some block reaches while other experts in the same block get fewer rows; each row names 2 different experts.
All inputs are finite; a program needn't handle non-finite values.
Results may differ from a plain program's by a relative error of at most 0.023.
Values may be sent and summed in bfloat16 or wider, within the bound.
A program may use at most 192 MiB of HBM per device.

v0:
```python
import jax
import jax.numpy as jnp
from jax import lax
from jax.sharding import PartitionSpec as P

SEGMENT = 64
SEQUENCES = 1
EPS = 1e-06
NEG = -1e30
CLAMP = 7.0
ALPHA = 1.702
OUT_FACTOR = 0.8


def shards(
    queries,
    key_vectors,
    values,
    head_lambda,
    head_gain,
    w_out,
    residual,
    ffn_gain,
    route_ids,
    route_logits,
    w_gate,
    w_up,
    w_down,
):
    tok_count = queries.shape[0]
    local_heads = head_lambda.shape[0]
    head_width = queries.shape[1] // (2 * local_heads)
    value_width = values.shape[1] // local_heads
    score_scale = head_width ** (-0.5)
    n_tp = lax.axis_size("tp")
    n_sp = lax.axis_size("sp")
    seq_length = tok_count * n_sp // SEQUENCES
    query_pos = lax.axis_index("sp") * tok_count + jnp.arange(tok_count, dtype=jnp.int32)
    query_seg = query_pos // SEGMENT
    query_seq = query_pos // seq_length
    seq_begin = query_seq[0] * seq_length
    last_seg = query_seg[tok_count - 1]
    query_heads = queries.reshape(tok_count, local_heads, 2, head_width)

    def absorb(carry, key_block, value_block, key_start):
        maxima, totals, sums = carry
        block_len = key_block.shape[0]
        key_pos = key_start + jnp.arange(block_len, dtype=jnp.int32)
        visible = ((key_pos // SEGMENT)[None, :] <= query_seg[:, None]) & (
            (key_pos // seq_length)[None, :] == query_seq[:, None]
        )
        score = (
            jnp.einsum(
                "qhjd,khjd->jhqk", query_heads, key_block, preferred_element_type=jnp.float32
            )
            * score_scale
        )
        score = jnp.where(visible, score, NEG)
        new_max = jnp.maximum(maxima, jnp.max(score, axis=-1))
        expo = jnp.where(visible, jnp.exp(score - new_max[..., None]), 0.0)
        factor = jnp.exp(maxima - new_max)
        totals = totals * factor + jnp.sum(expo, axis=-1)
        added = jnp.einsum(
            "jhqk,khd->jqhd",
            expo.astype(jnp.bfloat16),
            value_block,
            preferred_element_type=jnp.float32,
        )
        sums = sums * jnp.transpose(factor, (0, 2, 1))[..., None] + added
        return (new_max, totals, sums)

    def maybe_absorb(carry, key_block, value_block, key_start):
        block_len = key_block.shape[0]
        needed = (key_start // SEGMENT <= last_seg) & (key_start + block_len - 1 >= seq_begin)
        return lax.cond(
            needed,
            lambda inner: absorb(inner, key_block, value_block, key_start),
            lambda inner: inner,
            carry,
        )

    initial = (
        jnp.full((2, local_heads, tok_count), NEG, jnp.float32),
        jnp.zeros((2, local_heads, tok_count), jnp.float32),
        jnp.zeros((2, tok_count, local_heads, value_width), jnp.float32),
    )
    key_piece = lax.all_gather(key_vectors, "sp", axis=0, tiled=True)
    value_piece = lax.all_gather(values, "sp", axis=0, tiled=True)
    piece_len = key_piece.shape[0]
    key_rows = key_piece.reshape(piece_len, local_heads, 2, head_width)
    value_rows = value_piece.reshape(piece_len, local_heads, value_width)
    key_step = 512

    def advance(block_index, inner):
        key_offset = block_index * key_step
        key_block = lax.dynamic_slice_in_dim(key_rows, key_offset, key_step, 0)
        value_block = lax.dynamic_slice_in_dim(value_rows, key_offset, key_step, 0)
        return maybe_absorb(inner, key_block, value_block, key_offset)

    maxima, totals, sums = lax.fori_loop(0, piece_len // key_step, advance, initial)
    attended = sums / jnp.transpose(totals, (0, 2, 1))[..., None]
    diff = attended[0] - head_lambda[None, :, None] * attended[1]
    scale_rows = lax.rsqrt(jnp.mean(diff * diff, axis=-1, keepdims=True) + EPS)
    head_rows = (diff * scale_rows * head_gain * OUT_FACTOR).astype(jnp.bfloat16)
    head_rows = head_rows.reshape(tok_count, local_heads * value_width)
    own_count = tok_count // n_tp
    whole_weight = lax.all_gather(w_out, "tp", axis=0, tiled=True)
    token_heads = lax.all_to_all(head_rows, "tp", split_axis=0, concat_axis=1, tiled=True)
    projected = jnp.dot(token_heads, whole_weight, preferred_element_type=jnp.float32)
    mixed = (residual.astype(jnp.float32) + projected).astype(jnp.bfloat16)
    mixed32 = mixed.astype(jnp.float32)
    normed = (
        mixed32 * lax.rsqrt(jnp.mean(mixed32 * mixed32, axis=-1, keepdims=True) + EPS) * ffn_gain
    ).astype(jnp.bfloat16)
    gates = jax.nn.softmax(route_logits, axis=-1)
    top_count = route_ids.shape[1]
    model_width = normed.shape[1]
    cap_slots = max(2, 5 * top_count * tok_count // (4 * n_tp * n_sp))
    flat_ids = route_ids.reshape(-1)
    chosen = (flat_ids[:, None] == jnp.arange(n_sp, dtype=jnp.int32)[None, :]).astype(jnp.int32)
    earlier = jnp.cumsum(chosen, axis=0) - chosen
    slot_rank = jnp.sum(earlier * chosen, axis=1)
    slot_index = flat_ids * cap_slots + slot_rank
    source_rows = jnp.repeat(normed, top_count, axis=0)
    outgoing = (
        jnp.zeros((n_sp * cap_slots, model_width), jnp.bfloat16).at[slot_index].set(source_rows)
    )
    outgoing = outgoing.reshape(n_sp, cap_slots, model_width)
    arrived = lax.all_to_all(outgoing, "sp", split_axis=0, concat_axis=0, tiled=True)
    senders, slot_count, arrived_width = arrived.shape
    flat_in = arrived.reshape(senders * slot_count, arrived_width)
    piece = lax.all_gather(flat_in, "tp", axis=0, tiled=True)
    gate_pre = jnp.dot(piece, w_gate[0], preferred_element_type=jnp.float32)
    up_pre = jnp.dot(piece, w_up[0], preferred_element_type=jnp.float32)
    gate_cut = jnp.minimum(gate_pre, CLAMP)
    up_cut = jnp.clip(up_pre, -CLAMP, CLAMP)
    active = (gate_cut * jax.nn.sigmoid(ALPHA * gate_cut) * (up_cut + 1.0)).astype(jnp.bfloat16)
    reduced = lax.psum_scatter(
        jnp.dot(active, w_down[0], preferred_element_type=jnp.float32).astype(jnp.bfloat16),
        "tp",
        scatter_dimension=0,
        tiled=True,
    )
    reduced = reduced.reshape(senders, slot_count, arrived_width)
    returned = lax.all_to_all(reduced, "sp", split_axis=0, concat_axis=0, tiled=True)
    picked = returned.reshape(n_sp * cap_slots, model_width)[slot_index].astype(jnp.float32)
    weighted = (picked * gates.reshape(-1)[:, None]).reshape(own_count, top_count, model_width)
    return (mixed32 + jnp.sum(weighted, axis=1)).astype(jnp.bfloat16)


def solution(mesh):
    in_specs = (
        P("sp", "tp"),
        P("sp", "tp"),
        P("sp", "tp"),
        P("tp"),
        P(),
        P("tp", None),
        P(("sp", "tp"), None),
        P(),
        P(("sp", "tp"), None),
        P(("sp", "tp"), None),
        P("sp", None, "tp"),
        P("sp", None, "tp"),
        P("sp", "tp", None),
    )
    out_specs = P(("sp", "tp"), None)
    return jax.shard_map(shards, mesh=mesh, in_specs=in_specs, out_specs=out_specs, check_vma=False)
```

profile of v0, /device:TPU:0, one launch (start us, length us, event | category | flops | bytes accessed | tf_op | source)
XLA Modules:
  0.0 338.7 jit_solution(3574506045380296739)
XLA Ops:
  6.6 1.9 copy.37
  8.6 1.8 copy.39
  14.6 42.0 %all-gather.5.cloned.1.call-done = bf16[3072,256]{0,1:T(8,128)(2,1)} async-done(((bf16[384,256]{0,1:T(8,128)(2,1)}), bf16[3072,256]{0,1:T(8,128)(2,1)}) %all-gather.5.cloned.1.call-update) | async-done | bytes 1572880 | tf_op jit(solution)/shard_map/all_gather | solution.py:87
  56.6 2.7 copy.40
  59.3 42.0 %all-gather.7.cloned.1.call-done = bf16[3072,256]{0,1:T(8,128)(2,1)} async-done(((bf16[384,256]{0,1:T(8,128)(2,1)}), bf16[3072,256]{0,1:T(8,128)(2,1)}) %all-gather.7.cloned.1.call-update) | async-done | bytes 1572880 | tf_op jit(solution)/shard_map/all_gather | solution.py:88
  101.3 2.6 copy.42
  104.0 9.5 %while.24 = (s32[]{:T(128)}, f32[2,2,384]{2,1,0:T(2,128)S(1)}, f32[2,2,384]{2,1,0:T(2,128)S(1)}, f32[2,384,2,128]{3,1,0,2:T(8,128)S(1)}, s32[]{:T(128)}, /*index...) while((s32[]{:T(128)}, f32[2,2,384]{2,1,0:T(2,128)S(1)}, ...), condition=%wide.region_5.6_spmd.clone.clone, body=%wide.region_0.5_spmd.clone.clone.sunk | while | flops 310077472 | bytes 12468234 | solution.py:100
  104.7 4.9 %conditional.4 = ((f32[2,2,384]{2,1,0:T(2,128)S(1)}, f32[2,2,384]{2,1,0:T(2,128)S(1)}, f32[2,384,2,128]{3,1,0,2:T(8,128)S(1)})) conditional(s32[]{:T(128)} %convert_element_type.87, (f32[2,2,384]{2,1,0:T(2,128)S(1)}, f32[2,2,384]{2,1,0:T(2,128)S(1)}, f32[2,384,2,128]{3,1,0,2:T(8,128)S(1)}) %tuple.101, (s32[]{:T(128)}, ...), branch_computations={%region_1.1_spmd, %region_2.4_spmd.clone} | conditional | flops 310070912 | bytes 12456133 | solution.py:75
  105.1 1.7 fusion.4
  107.7 1.9 fusion.12
  116.8 1.3 copy.46
  120.4 1.8 multiply_convert_fusion.2
  122.2 3.4 all-to-all-start
  125.6 7.7 %all-to-all-done = bf16[4,96,256]{2,1,0:T(8,128)(2,1)S(1)} async-done(((bf16[4,96,256]{2,1,0:T(8,128)(2,1)}), bf16[4,96,256]{2,1,0:T(8,128)(2,1)S(1)}, u32[]{:S(2)}, u32[]{:S(2)}) %all-to-all-start) | async-done | bytes 196640 | tf_op jit(solution)/shard_map/all_to_all | solution.py:108
  133.3 4.3 %all-gather.9.cloned.1.call-done = bf16[1024,2048]{1,0:T(8,128)(2,1)} async-done(((bf16[256,2048]{1,0:T(8,128)(2,1)}), bf16[1024,2048]{1,0:T(8,128)(2,1)}) %all-gather.9.cloned.1.call-update) | async-done | bytes 4194320 | tf_op jit(solution)/shard_map/all_gather | solution.py:107
  137.6 3.2 multiply_reduce_fusion.1
  142.4 1.2 reshape.176
  143.6 3.3 scatter_custom_fusion
  146.9 1.5 reshape.158
  148.4 45.5 %all_to_all.26 = bf16[8,30,2048]{2,1,0:T(8,128)(2,1)} all-to-all(bf16[8,30,2048]{2,1,0:T(8,128)(2,1)S(1)} %reshape.158), channel_id=1, replica_groups=mesh['sp'=8,'tp'=4] {'sp'}, dimensions={0} | all-to-all | bytes 1966080 | tf_op jit(solution)/shard_map/all_to_all | solution.py:129
  193.9 2.4 reshape.159
  196.6 31.4 %all-gather.11.cloned.1.call-done = bf16[960,2048]{1,0:T(8,128)(2,1)} async-done(((bf16[240,2048]{1,0:T(8,128)(2,1)}), bf16[960,2048]{1,0:T(8,128)(2,1)}) %all-gather.11.cloned.1.call-update) | async-done | bytes 3932176 | tf_op jit(solution)/shard_map/all_gather | solution.py:132
  228.0 6.3 %fusion.35 = f32[960,512]{1,0:T(8,128)} fusion(bf16[960,2048]{1,0:T(8,128)(2,1)} %all-gather.11.cloned.1.call-done, bf16[1,2048,512]{2,1,0:T(8,128)(2,1)} %param.28), kind=kOutput, calls=%fused_computation.54 | convolution fusion | flops 2013265920 | bytes 7995392 | tf_op jit(solution)/shard_map/dot_general | solution.py:134
  234.4 9.8 %convolution_convert_fusion = bf16[960,2048]{1,0:T(8,128)(2,1)} fusion(bf16[1,512,2048]{2,1,0:T(8,128)(2,1)S(1)} %copy-done, f32[960,512]{1,0:T(8,128)} %fusion.35, bf16[960,2048]{1,0:T(8,128)(2,1)} %all-gather.11.cloned.1.call-done, bf16[1,2048,512]{2,1,0:T(8,128)(2,1)} %param.27), kind=kOutput, calls=%fused_computation.49 | convolution fusion | flops 4033413120 | bytes 14024704 | tf_op jit(solution)/shard_map/dot_general | solution.py:139
  244.3 43.0 %reduce-scatter.2.cloned.1.call-done = bf16[240,2048]{1,0:T(8,128)(2,1)} async-done(((bf16[960,2048]{1,0:T(8,128)(2,1)}), bf16[240,2048]{1,0:T(8,128)(2,1)}) %reduce-scatter.2.cloned.1.call-update) | async-done | bytes 983056 | tf_op jit(solution)/shard_map/reduce_scatter | solution.py:138
  287.3 2.4 reshape.160
  289.7 5.5 %all-to-all-start.2 = ((bf16[8,30,2048]{2,1,0:T(8,128)(2,1)}), bf16[8,30,2048]{2,1,0:T(8,128)(2,1)}, u32[]{:S(2)}, u32[]{:S(2)}) async-start(bf16[8,30,2048]{2,1,0:T(8,128)(2,1)} %reshape.160), calls=%async_computation.3 | async-start | bytes 2097152 | tf_op jit(solution)/shard_map/all_to_all | solution.py:145
  295.4 25.6 %all-to-all-done.2 = bf16[8,30,2048]{2,1,0:T(8,128)(2,1)} async-done(((bf16[8,30,2048]{2,1,0:T(8,128)(2,1)}), bf16[8,30,2048]{2,1,0:T(8,128)(2,1)}, u32[]{:S(2)}, u32[]{:S(2)}) %all-to-all-start.2) | async-done | bytes 983072 | tf_op jit(solution)/shard_map/all_to_all | solution.py:145
  321.0 1.5 reshape.161
  322.5 2.0 gather_fusion
  324.5 3.0 reshape.163
  327.6 3.7 %multiply_reduce_fusion = f32[96,2048]{1,0:T(8,128)S(1)} fusion(f32[96,2,2048]{2,1,0:T(2,128)} %reshape.163, f32[96,2]{1,0:T(8,128)S(1)} %copy.51), kind=kLoop, calls=%fused_computation.59 | loop fusion | flops 589824 | bytes 2360064 | tf_op jit(solution)/shard_map/reduce_sum | solution.py:148
  (127 shorter events, 13.8 us)
Async XLA Ops:
  6.5 227.8 %copy-start = (bf16[1,512,2048]{2,1,0:T(8,128)(2,1)S(1)}, bf16[1,512,2048]{2,1,0:T(8,128)(2,1)}, u32[]{:S(2)}) copy-start(bf16[1,512,2048]{2,1,0:T(8,128)(2,1)} %param.29) | copy-start | bytes 6291460
  6.5 5.7 %copy-start.6 = (bf16[384,256]{1,0:T(8,128)(2,1)S(1)}, bf16[384,256]{1,0:T(8,128)(2,1)}, u32[]{:S(2)}) copy-start(bf16[384,256]{1,0:T(8,128)(2,1)} %param.17) | copy-start | bytes 589828
  6.5 5.9 %copy-start.9 = (s32[96,2]{0,1:T(2,128)S(1)}, s32[96,2]{0,1:T(2,128)}, u32[]{:S(2)}) copy-start(s32[96,2]{0,1:T(2,128)} %param.25) | copy-start | bytes 2308
  6.5 8.0 %copy-start.10 = (f32[2]{0:T(128)S(1)}, f32[2]{0:T(128)}, u32[]{:S(2)}) copy-start(f32[2]{0:T(128)} %param.20) | copy-start | bytes 28
  6.5 8.0 %copy-start.11 = (f32[128]{0:T(128)S(1)}, f32[128]{0:T(128)}, u32[]{:S(2)}) copy-start(f32[128]{0:T(128)} %param.21) | copy-start | bytes 1540
  6.5 50.0 %all-gather.5.cloned.1.call-start = ((), (), s32[]{:S(2)}) async-start(), calls=%async_computation.4 | async-start | bytes 1769472 | tf_op jit(solution)/shard_map/all_gather | solution.py:87
  8.5 92.8 %all-gather.7.cloned.1.call-start = ((), (), s32[]{:S(2)}) async-start(), calls=%async_computation.5 | async-start | bytes 1769472 | tf_op jit(solution)/shard_map/all_gather | solution.py:88
  10.3 127.3 %all-gather.9.cloned.1.call-start = ((), (), s32[]{:S(2)}) async-start(), calls=%async_computation.6 | async-start | bytes 5242880 | tf_op jit(solution)/shard_map/all_gather | solution.py:107
  113.7 0.9 copy-start.1
  115.4 3.8 %copy-start.2 = (f32[2,384,2,128]{3,1,0,2:T(8,128)S(1)}, f32[2,384,2,128]{3,1,0,2:T(8,128)}, u32[]{:S(2)}) copy-start(f32[2,384,2,128]{3,1,0,2:T(8,128)} %copy-done.1) | copy-start | bytes 2359300
  119.2 1.2 copy-start.5
  122.2 11.2 %all-to-all-start = ((bf16[4,96,256]{2,1,0:T(8,128)(2,1)}), bf16[4,96,256]{2,1,0:T(8,128)(2,1)S(1)}, u32[]{:S(2)}, u32[]{:S(2)}) async-start(bf16[4,96,256]{2,1,0:T(8,128)(2,1)} %multiply_convert_fusion.2), calls=%async_computation | async-start | bytes 393216 | tf_op jit(solution)/shard_map/all_to_all | solution.py:108
  125.5 102.5 %all-gather.11.cloned.1.call-start = ((), (), s32[]{:S(2)}) async-start(), calls=%async_computation.7 | async-start | bytes 4915200 | tf_op jit(solution)/shard_map/all_gather | solution.py:132
  137.6 4.1 %copy-start.8 = (f32[2048]{0:T(1024)S(1)}, f32[2048]{0:T(1024)}, u32[]{:S(2)}) copy-start(f32[2048]{0:T(1024)} %param.24) | copy-start | bytes 24580
  140.8 0.9 copy-start.3
  196.4 90.9 %reduce-scatter.2.cloned.1.call-start = ((), (), s32[]{:S(2)}) async-start(), calls=%async_computation.8 | async-start | bytes 4915200 | tf_op jit(solution)/shard_map/reduce_scatter | solution.py:138
  244.2 51.0 %copy-start.7 = (f32[96,2]{0,1:T(2,128)S(1)}, f32[96,2]{0,1:T(2,128)}, u32[]{:S(2)}) copy-start(f32[96,2]{0,1:T(2,128)} %param.26) | copy-start | bytes 2308
  289.7 31.3 %all-to-all-start.2 = ((bf16[8,30,2048]{2,1,0:T(8,128)(2,1)}), bf16[8,30,2048]{2,1,0:T(8,128)(2,1)}, u32[]{:S(2)}, u32[]{:S(2)}) async-start(bf16[8,30,2048]{2,1,0:T(8,128)(2,1)} %reshape.160), calls=%async_computation.3 | async-start | bytes 2097152 | tf_op jit(solution)/shard_map/all_to_all | solution.py:145
  324.5 6.8 %copy-start.4 = (f32[96,2048]{1,0:T(8,128)S(1)}, f32[96,2048]{1,0:T(8,128)}, u32[]{:S(2)}) copy-start(f32[96,2048]{1,0:T(8,128)} %copy-done.3) | copy-start | bytes 2359300
Sparse Core Ops, SparseCore 0:
  9.4 47.1 all-gather.4
  58.6 42.5 all-gather.6
  102.9 34.7 all-gather.8
  196.5 31.4 all-gather.10
  244.4 42.8 reduce-scatter.1
where the time goes:
time: 340 us; the launch traced here: 339 us
  waiting for transfers between devices  197 us (58%)
  blocking collectives  45.5 us (13%)
  local copies, waits for them, and re-layouts  36.4 us (11%)
  matrix products  22.9 us (7%)
  between operations  14.1 us (4%)
  starting transfers between devices  9.27 us (3%)
  other arithmetic  9.27 us (3%)
  loops' own time  4.41 us (1%)
    all_to_all x1, blocking collectives, shards(): lax.all_to_all(outgoing, 'sp', split_axis=0, concat_axis=0, tiled=True)  45.5 us
    reduce_scatter x1, waiting for transfers between devices, shards(): lax.psum_scatter(jnp.dot(active, w_down[0], preferred_element_type=jnp.fl...  43 us
    all_gather x1, waiting for transfers between devices, shards(): value_piece = lax.all_gather(values, 'sp', axis=0, tiled=True)  42 us
    all_gather x1, waiting for transfers between devices, shards(): key_piece = lax.all_gather(key_vectors, 'sp', axis=0, tiled=True)  42 us
    all_gather x1, waiting for transfers between devices, shards(): piece = lax.all_gather(flat_in, 'tp', axis=0, tiled=True)  31.4 us
    all_to_all x1, waiting for transfers between devices, shards(): lax.all_to_all(reduced, 'sp', split_axis=0, concat_axis=0, tiled=True)  25.6 us
    unnamed x31, local copies, waits for them, and re-layouts  11 us
    dot_general x1, matrix products, shards(): jnp.dot(active, w_down[0], preferred_element_type=jnp.float32)  9.84 us
  transfers between devices with their start and end apart: 7, of which 7 were waited for; matrix products, arithmetic and copies ran while one was open for 7% of the time, Pallas kernels for 0%

commit v1 on v0

--- a/solution.py
+++ b/solution.py
@@ -85,7 +85,12 @@
         jnp.zeros((2, tok_count, local_heads, value_width), jnp.float32),
     )
     key_piece = lax.all_gather(key_vectors, "sp", axis=0, tiled=True)
-    value_piece = lax.all_gather(values, "sp", axis=0, tiled=True)
+    ring = [values]
+    for hop in range(7):
+        ring.append(lax.ppermute(ring[-1], "sp", [(dev, (dev + 1) % 8) for dev in range(8)]))
+    value_piece = jnp.roll(
+        jnp.concatenate(ring[::-1], axis=0), (lax.axis_index("sp") + 1) * ring[0].shape[0], axis=0
+    )
     piece_len = key_piece.shape[0]
     key_rows = key_piece.reshape(piece_len, local_heads, 2, head_width)
     value_rows = value_piece.reshape(piece_len, local_heads, value_width)

time: 340 us -> 330 us (0.971)
  waiting for transfers between devices: 197 us -> 171 us
  local copies, waits for them, and re-layouts: 36.4 us -> 43.2 us
  blocking collectives: 45.5 us -> 50.6 us
    ppermute x0 -> x7, waiting for transfers between devices: none -> 65.3 us  [shards(): lax.ppermute(ring[-1], 'sp', [(dev, (dev + 1) % 8) for dev in range(8)])]
    all_gather x1 -> x0, waiting for transfers between devices: 42 us -> none  [shards(): value_piece = lax.all_gather(values, 'sp', axis=0, tiled=True)]
    all_gather x1, waiting for transfers between devices: 42 us -> 0.01 us  [shards(): key_piece = lax.all_gather(key_vectors, 'sp', axis=0, tiled=True)]
    all_to_all x1, blocking collectives: 45.5 us -> 50.6 us  [shards(): lax.all_to_all(outgoing, 'sp', split_axis=0, concat_axis=0, tiled=True)]
    unnamed x31 -> x42, local copies, waits for them, and re-layouts: 11 us -> 15.9 us
    all_gather x1, waiting for transfers between devices: 4.3 us -> 0.02 us  [shards(): whole_weight = lax.all_gather(w_out, 'tp', axis=0, tiled=True)]
  transfers between devices with their start and end apart: 7 -> 13, of which waited for: 7 -> 11; matrix products, arithmetic and copies ran while one was open for 7% -> 9% of each run, Pallas kernels for 0% -> 0%
where the time goes in v1:
time: 330 us; the launch traced here: 328 us
  waiting for transfers between devices  171 us (52%)
  blocking collectives  50.6 us (15%)
  local copies, waits for them, and re-layouts  43.2 us (13%)
  matrix products  22.8 us (7%)
  between operations  14.1 us (4%)
  starting transfers between devices  12.4 us (4%)
  other arithmetic  10.1 us (3%)
  loops' own time  4.4 us (1%)
    ppermute x7, waiting for transfers between devices, shards(): lax.ppermute(ring[-1], 'sp', [(dev, (dev + 1) % 8) for dev in range(8)])  65.3 us
    all_to_all x1, blocking collectives, shards(): lax.all_to_all(outgoing, 'sp', split_axis=0, concat_axis=0, tiled=True)  50.6 us
    reduce_scatter x1, waiting for transfers between devices, shards(): lax.psum_scatter(jnp.dot(active, w_down[0], preferred_element_type=jnp.fl...  43.1 us
    all_gather x1, waiting for transfers between devices, shards(): piece = lax.all_gather(flat_in, 'tp', axis=0, tiled=True)  31.6 us
    all_to_all x1, waiting for transfers between devices, shards(): lax.all_to_all(reduced, 'sp', split_axis=0, concat_axis=0, tiled=True)  25.6 us
    unnamed x42, local copies, waits for them, and re-layouts  15.9 us
    dot_general x1, matrix products, shards(): jnp.dot(active, w_down[0], preferred_element_type=jnp.float32)  9.83 us
  transfers between devices with their start and end apart: 13, of which 11 were waited for; matrix products, arithmetic and copies ran while one was open for 9% of the time, Pallas kernels for 0%

profile of v1, /device:TPU:0, one launch (start us, length us, event | category | flops | bytes accessed | tf_op | source)
XLA Modules:
  0.0 328.2 jit_solution(12206187334356444840)
XLA Ops:
  6.5 1.9 copy.39
  9.6 3.0 collective-permute-start
  13.6 7.0 %collective-permute-done = bf16[384,256]{0,1:T(8,128)(2,1)S(1)} collective-permute-done((bf16[384,256]{0,1:T(8,128)(2,1)S(1)}, bf16[384,256]{0,1:T(8,128)(2,1)S(1)}, u32[]{:S(2)}, u32[]{:S(2)}) %collective-permute-start) | collective-permute-done | bytes 196640 | tf_op jit(solution)/shard_map/ppermute | solution.py:90
  20.6 12.6 %collective-permute-done.1 = bf16[384,256]{0,1:T(8,128)(2,1)S(1)} collective-permute-done((bf16[384,256]{0,1:T(8,128)(2,1)S(1)}, bf16[384,256]{0,1:T(8,128)(2,1)S(1)}, u32[]{:S(2)}, u32[]{:S(2)}) %collective-permute-start.1) | collective-permute-done | bytes 196640 | tf_op jit(solution)/shard_map/ppermute | solution.py:90
  34.0 7.5 %collective-permute-done.2 = bf16[384,256]{0,1:T(8,128)(2,1)S(1)} collective-permute-done((bf16[384,256]{0,1:T(8,128)(2,1)S(1)}, bf16[384,256]{0,1:T(8,128)(2,1)S(1)}, u32[]{:S(2)}, u32[]{:S(2)}) %collective-permute-start.2) | collective-permute-done | bytes 196640 | tf_op jit(solution)/shard_map/ppermute | solution.py:90
  41.6 13.4 %collective-permute-done.3 = bf16[384,256]{0,1:T(8,128)(2,1)S(1)} collective-permute-done((bf16[384,256]{0,1:T(8,128)(2,1)S(1)}, bf16[384,256]{0,1:T(8,128)(2,1)S(1)}, u32[]{:S(2)}, u32[]{:S(2)}) %collective-permute-start.3) | collective-permute-done | bytes 196640 | tf_op jit(solution)/shard_map/ppermute | solution.py:90
  55.7 10.8 %collective-permute-done.4 = bf16[384,256]{0,1:T(8,128)(2,1)S(1)} collective-permute-done((bf16[384,256]{0,1:T(8,128)(2,1)S(1)}, bf16[384,256]{0,1:T(8,128)(2,1)S(1)}, u32[]{:S(2)}, u32[]{:S(2)}) %collective-permute-start.4) | collective-permute-done | bytes 196640 | tf_op jit(solution)/shard_map/ppermute | solution.py:90
  71.3 5.5 %collective-permute-done.5 = bf16[384,256]{0,1:T(8,128)(2,1)} collective-permute-done((bf16[384,256]{0,1:T(8,128)(2,1)S(1)}, bf16[384,256]{0,1:T(8,128)(2,1)}, u32[]{:S(2)}, u32[]{:S(2)}) %collective-permute-start.5) | collective-permute-done | bytes 196640 | tf_op jit(solution)/shard_map/ppermute | solution.py:90
  76.8 8.5 %collective-permute-done.6 = bf16[384,256]{0,1:T(8,128)(2,1)S(1)} collective-permute-done((bf16[384,256]{0,1:T(8,128)(2,1)}, bf16[384,256]{0,1:T(8,128)(2,1)S(1)}, u32[]{:S(2)}, u32[]{:S(2)}) %collective-permute-start.6) | collective-permute-done | bytes 196640 | tf_op jit(solution)/shard_map/ppermute | solution.py:90
  87.9 1.8 constant_dynamic-slice_fusion
  89.7 2.6 copy.46
  92.3 2.7 copy.44
  95.1 9.4 %while.24 = (s32[]{:T(128)}, f32[2,2,384]{2,1,0:T(2,128)S(1)}, f32[2,2,384]{2,1,0:T(2,128)S(1)}, f32[2,384,2,128]{3,1,0,2:T(8,128)S(1)}, s32[]{:T(128)}, /*index...) while((s32[]{:T(128)}, f32[2,2,384]{2,1,0:T(2,128)S(1)}, ...), condition=%wide.region_5.6_spmd.clone.clone, body=%wide.region_0.5_spmd.clone.clone.sunk | while | flops 310077472 | bytes 12468234 | solution.py:105
  95.8 4.9 %conditional.4 = ((f32[2,2,384]{2,1,0:T(2,128)S(1)}, f32[2,2,384]{2,1,0:T(2,128)S(1)}, f32[2,384,2,128]{3,1,0,2:T(8,128)S(1)})) conditional(s32[]{:T(128)} %convert_element_type.87, (f32[2,2,384]{2,1,0:T(2,128)S(1)}, f32[2,2,384]{2,1,0:T(2,128)S(1)}, f32[2,384,2,128]{3,1,0,2:T(8,128)S(1)}) %tuple.101, (s32[]{:T(128)}, ...), branch_computations={%region_1.1_spmd, %region_2.4_spmd.clone} | conditional | flops 310070912 | bytes 12456133 | solution.py:75
  98.8 1.9 fusion.12
  111.5 1.9 multiply_convert_fusion.2
  113.4 3.5 %all-to-all-start = ((bf16[4,96,256]{2,1,0:T(8,128)(2,1)}), bf16[4,96,256]{2,1,0:T(8,128)(2,1)S(1)}, u32[]{:S(2)}, u32[]{:S(2)}) async-start(bf16[4,96,256]{2,1,0:T(8,128)(2,1)} %multiply_convert_fusion.2), calls=%async_computation | async-start | bytes 393216 | tf_op jit(solution)/shard_map/all_to_all | solution.py:113
  117.1 5.0 %all-to-all-done = bf16[4,96,256]{2,1,0:T(8,128)(2,1)S(1)} async-done(((bf16[4,96,256]{2,1,0:T(8,128)(2,1)}), bf16[4,96,256]{2,1,0:T(8,128)(2,1)S(1)}, u32[]{:S(2)}, u32[]{:S(2)}) %all-to-all-start) | async-done | bytes 196640 | tf_op jit(solution)/shard_map/all_to_all | solution.py:113
  122.2 3.1 multiply_reduce_fusion.1
  128.0 3.3 %scatter_custom_fusion = bf16[240,2048]{1,0:T(8,128)(2,1)} fusion(s32[192]{0:T(256)S(1)} %bitcast.84, bf16[192,2048]{1,0:T(8,128)(2,1)} %reshape.176, bf16[]{:T(256)} %constant.252.clone.1), kind=kCustom, calls=%fused_computation.63 | custom fusion | bytes 983552 | tf_op jit(solution)/shard_map/scatter | solution.py:131
  132.9 50.6 %all_to_all.26 = bf16[8,30,2048]{2,1,0:T(8,128)(2,1)} all-to-all(bf16[8,30,2048]{2,1,0:T(8,128)(2,1)S(1)} %reshape.158), channel_id=1, replica_groups=mesh['sp'=8,'tp'=4] {'sp'}, dimensions={0} | all-to-all | bytes 1966080 | tf_op jit(solution)/shard_map/all_to_all | solution.py:134
  183.4 2.4 reshape.159
  186.0 31.6 %all-gather.8.cloned.1.call-done = bf16[960,2048]{1,0:T(8,128)(2,1)} async-done(((bf16[240,2048]{1,0:T(8,128)(2,1)}), bf16[960,2048]{1,0:T(8,128)(2,1)}) %all-gather.8.cloned.1.call-update) | async-done | bytes 3932176 | tf_op jit(solution)/shard_map/all_gather | solution.py:137
  217.5 6.3 %fusion.35 = f32[960,512]{1,0:T(8,128)} fusion(bf16[960,2048]{1,0:T(8,128)(2,1)} %all-gather.8.cloned.1.call-done, bf16[1,2048,512]{2,1,0:T(8,128)(2,1)} %param.28), kind=kOutput, calls=%fused_computation.54 | convolution fusion | flops 2013265920 | bytes 7995392 | tf_op jit(solution)/shard_map/dot_general | solution.py:139
  223.9 9.8 %convolution_convert_fusion = bf16[960,2048]{1,0:T(8,128)(2,1)} fusion(bf16[1,512,2048]{2,1,0:T(8,128)(2,1)S(1)} %copy-done, f32[960,512]{1,0:T(8,128)} %fusion.35, bf16[960,2048]{1,0:T(8,128)(2,1)} %all-gather.8.cloned.1.call-done, bf16[1,2048,512]{2,1,0:T(8,128)(2,1)} %param.27), kind=kOutput, calls=%fused_computation.49 | convolution fusion | flops 4033413120 | bytes 14024704 | tf_op jit(solution)/shard_map/dot_general | solution.py:144
  233.7 43.1 %reduce-scatter.2.cloned.1.call-done = bf16[240,2048]{1,0:T(8,128)(2,1)} async-done(((bf16[960,2048]{1,0:T(8,128)(2,1)}), bf16[240,2048]{1,0:T(8,128)(2,1)}) %reduce-scatter.2.cloned.1.call-update) | async-done | bytes 983056 | tf_op jit(solution)/shard_map/reduce_scatter | solution.py:143
  276.8 2.4 reshape.160
  279.3 5.5 %all-to-all-start.2 = ((bf16[8,30,2048]{2,1,0:T(8,128)(2,1)}), bf16[8,30,2048]{2,1,0:T(8,128)(2,1)}, u32[]{:S(2)}, u32[]{:S(2)}) async-start(bf16[8,30,2048]{2,1,0:T(8,128)(2,1)} %reshape.160), calls=%async_computation.3 | async-start | bytes 2097152 | tf_op jit(solution)/shard_map/all_to_all | solution.py:150
  285.0 25.6 %all-to-all-done.2 = bf16[8,30,2048]{2,1,0:T(8,128)(2,1)} async-done(((bf16[8,30,2048]{2,1,0:T(8,128)(2,1)}), bf16[8,30,2048]{2,1,0:T(8,128)(2,1)}, u32[]{:S(2)}, u32[]{:S(2)}) %all-to-all-start.2) | async-done | bytes 983072 | tf_op jit(solution)/shard_map/all_to_all | solution.py:150
  312.0 2.0 gather_fusion
  314.1 3.0 reshape.163
  317.1 3.7 %multiply_reduce_fusion = f32[96,2048]{1,0:T(8,128)S(1)} fusion(f32[96,2,2048]{2,1,0:T(2,128)} %reshape.163, f32[96,2]{1,0:T(8,128)S(1)} %copy.55), kind=kLoop, calls=%fused_computation.59 | loop fusion | flops 589824 | bytes 2360064 | tf_op jit(solution)/shard_map/reduce_sum | solution.py:153
  (151 shorter events, 27.6 us)
Async XLA Ops:
  6.5 217.4 %copy-start = (bf16[1,512,2048]{2,1,0:T(8,128)(2,1)S(1)}, bf16[1,512,2048]{2,1,0:T(8,128)(2,1)}, u32[]{:S(2)}) copy-start(bf16[1,512,2048]{2,1,0:T(8,128)(2,1)} %param.29) | copy-start | bytes 6291460
  6.5 70.2 %copy-start.8 = (f32[2]{0:T(128)S(1)}, f32[2]{0:T(128)}, u32[]{:S(2)}) copy-start(f32[2]{0:T(128)} %param.20) | copy-start | bytes 28
  6.5 70.2 %copy-start.9 = (f32[128]{0:T(128)S(1)}, f32[128]{0:T(128)}, u32[]{:S(2)}) copy-start(f32[128]{0:T(128)} %param.21) | copy-start | bytes 1540
  6.5 85.8 %all-gather.4.cloned.1.call-start = ((), (), s32[]{:S(2)}) async-start(), calls=%async_computation.4 | async-start | bytes 1769472 | tf_op jit(solution)/shard_map/all_gather | solution.py:87
  8.5 113.7 %all-gather.6.cloned.1.call-start = ((), (), s32[]{:S(2)}) async-start(), calls=%async_computation.5 | async-start | bytes 5242880 | tf_op jit(solution)/shard_map/all_gather | solution.py:112
  9.6 11.0 %collective-permute-start = (bf16[384,256]{0,1:T(8,128)(2,1)S(1)}, bf16[384,256]{0,1:T(8,128)(2,1)S(1)}, u32[]{:S(2)}, u32[]{:S(2)}) collective-permute-start(bf16[384,256]{0,1:T(8,128)(2,1)S(1)} %copy.41), channel_id=1, source_target_pairs={{0,4},{4,8},{8,12},{12,16},{16,20},{20,24},{24,28},{28,0},{1,5},{5... | collective-permute-start | bytes 589832 | tf_op jit(solution)/shard_map/ppermute | solution.py:90
  20.6 12.6 %collective-permute-start.1 = (bf16[384,256]{0,1:T(8,128)(2,1)S(1)}, bf16[384,256]{0,1:T(8,128)(2,1)S(1)}, u32[]{:S(2)}, u32[]{:S(2)}) collective-permute-start(bf16[384,256]{0,1:T(8,128)(2,1)S(1)} %collective-permute-done), channel_id=1, source_target_pairs={{0,4},{4,8},{8,12},{12,16},{16,20},{20,24},{24,28},{28,0},{1,5},{5... | collective-permute-start | bytes 589832 | tf_op jit(solution)/shard_map/ppermute | solution.py:90
  33.2 8.4 %collective-permute-start.2 = (bf16[384,256]{0,1:T(8,128)(2,1)S(1)}, bf16[384,256]{0,1:T(8,128)(2,1)S(1)}, u32[]{:S(2)}, u32[]{:S(2)}) collective-permute-start(bf16[384,256]{0,1:T(8,128)(2,1)S(1)} %collective-permute-done.1), channel_id=1, source_target_pairs={{0,4},{4,8},{8,12},{12,16},{16,20},{20,24},{24,28},{28,0},{1,5},{5... | collective-permute-start | bytes 589832 | tf_op jit(solution)/shard_map/ppermute | solution.py:90
  41.5 13.5 %collective-permute-start.3 = (bf16[384,256]{0,1:T(8,128)(2,1)S(1)}, bf16[384,256]{0,1:T(8,128)(2,1)S(1)}, u32[]{:S(2)}, u32[]{:S(2)}) collective-permute-start(bf16[384,256]{0,1:T(8,128)(2,1)S(1)} %collective-permute-done.2), channel_id=1, source_target_pairs={{0,4},{4,8},{8,12},{12,16},{16,20},{20,24},{24,28},{28,0},{1,5},{5... | collective-permute-start | bytes 589832 | tf_op jit(solution)/shard_map/ppermute | solution.py:90
  55.1 11.5 %collective-permute-start.4 = (bf16[384,256]{0,1:T(8,128)(2,1)S(1)}, bf16[384,256]{0,1:T(8,128)(2,1)S(1)}, u32[]{:S(2)}, u32[]{:S(2)}) collective-permute-start(bf16[384,256]{0,1:T(8,128)(2,1)S(1)} %collective-permute-done.3), channel_id=1, source_target_pairs={{0,4},{4,8},{8,12},{12,16},{16,20},{20,24},{24,28},{28,0},{1,5},{5... | collective-permute-start | bytes 589832 | tf_op jit(solution)/shard_map/ppermute | solution.py:90
  66.6 10.2 %collective-permute-start.5 = (bf16[384,256]{0,1:T(8,128)(2,1)S(1)}, bf16[384,256]{0,1:T(8,128)(2,1)}, u32[]{:S(2)}, u32[]{:S(2)}) collective-permute-start(bf16[384,256]{0,1:T(8,128)(2,1)S(1)} %collective-permute-done.4), channel_id=1, source_target_pairs={{0,4},{4,8},{8,12},{12,16},{16,20},{20,24},{24,28},{28,0},{1,5},{5... | collective-permute-start | bytes 589832 | tf_op jit(solution)/shard_map/ppermute | solution.py:90
  76.8 8.6 %collective-permute-start.6 = (bf16[384,256]{0,1:T(8,128)(2,1)}, bf16[384,256]{0,1:T(8,128)(2,1)S(1)}, u32[]{:S(2)}, u32[]{:S(2)}) collective-permute-start(bf16[384,256]{0,1:T(8,128)(2,1)} %collective-permute-done.5), channel_id=1, source_target_pairs={{0,4},{4,8},{8,12},{12,16},{16,20},{20,24},{24,28},{28,0},{1,5},{5... | collective-permute-start | bytes 589832 | tf_op jit(solution)/shard_map/ppermute | solution.py:90
  104.8 0.9 copy-start.1
  106.5 3.7 %copy-start.2 = (f32[2,384,2,128]{3,1,0,2:T(8,128)S(1)}, f32[2,384,2,128]{3,1,0,2:T(8,128)}, u32[]{:S(2)}) copy-start(f32[2,384,2,128]{3,1,0,2:T(8,128)} %copy-done.1) | copy-start | bytes 2359300
  110.3 11.9 %copy-start.5 = (bf16[96,2048]{1,0:T(8,128)(2,1)S(1)}, bf16[96,2048]{1,0:T(8,128)(2,1)}, u32[]{:S(2)}) copy-start(bf16[96,2048]{1,0:T(8,128)(2,1)} %param.23) | copy-start | bytes 1179652
  113.3 12.9 %copy-start.7 = (f32[2048]{0:T(1024)S(1)}, f32[2048]{0:T(1024)}, u32[]{:S(2)}) copy-start(f32[2048]{0:T(1024)} %param.24) | copy-start | bytes 24580
  113.4 8.8 %all-to-all-start = ((bf16[4,96,256]{2,1,0:T(8,128)(2,1)}), bf16[4,96,256]{2,1,0:T(8,128)(2,1)S(1)}, u32[]{:S(2)}, u32[]{:S(2)}) async-start(bf16[4,96,256]{2,1,0:T(8,128)(2,1)} %multiply_convert_fusion.2), calls=%async_computation | async-start | bytes 393216 | tf_op jit(solution)/shard_map/all_to_all | solution.py:113
  116.9 100.7 %all-gather.8.cloned.1.call-start = ((), (), s32[]{:S(2)}) async-start(), calls=%async_computation.6 | async-start | bytes 4915200 | tf_op jit(solution)/shard_map/all_gather | solution.py:137
  125.3 0.9 copy-start.3
  185.9 90.9 %reduce-scatter.2.cloned.1.call-start = ((), (), s32[]{:S(2)}) async-start(), calls=%async_computation.7 | async-start | bytes 4915200 | tf_op jit(solution)/shard_map/reduce_scatter | solution.py:143
  233.7 51.1 %copy-start.6 = (f32[96,2]{0,1:T(2,128)S(1)}, f32[96,2]{0,1:T(2,128)}, u32[]{:S(2)}) copy-start(f32[96,2]{0,1:T(2,128)} %param.26) | copy-start | bytes 2308
  279.3 31.3 %all-to-all-start.2 = ((bf16[8,30,2048]{2,1,0:T(8,128)(2,1)}), bf16[8,30,2048]{2,1,0:T(8,128)(2,1)}, u32[]{:S(2)}, u32[]{:S(2)}) async-start(bf16[8,30,2048]{2,1,0:T(8,128)(2,1)} %reshape.160), calls=%async_computation.3 | async-start | bytes 2097152 | tf_op jit(solution)/shard_map/all_to_all | solution.py:150
  314.1 6.8 %copy-start.4 = (f32[96,2048]{1,0:T(8,128)S(1)}, f32[96,2048]{1,0:T(8,128)}, u32[]{:S(2)}) copy-start(f32[96,2048]{1,0:T(8,128)} %copy-done.3) | copy-start | bytes 2359300
Sparse Core Ops, SparseCore 0:
  9.4 54.1 all-gather.3
  65.1 35.0 all-gather.5
  186.0 31.4 all-gather.7
  233.9 42.9 reduce-scatter.1
